TPU v7x, 32 devices: a whole 2x2x4 slice. The times are simulated.
32 devices in a mesh: sp: 8 (over z, x), tp: 4 (over y, core).
Axes of the slice: x: 2, y: 2, z: 4, core: 2. Of those that a mesh axis runs over, the one named last changes fastest.
Arguments:
- query_proj: bfloat16 [4096, 1024], P('sp', 'tp'), may hold values from -6 to 6
- projected_keys: bfloat16 [4096, 512], P('sp', 'tp'), may hold values from -6 to 6
- projected_values: bfloat16 [4096, 512], P('sp', 'tp'), may hold values from -6 to 6
- residual: bfloat16 [4096, 2048], P(('sp', 'tp')), may hold values from -6 to 6
- out_weight: bfloat16 [1024, 2048], replicated, may hold values from -0.1875 to 0.1875
- mix_gain: float32 [2048], replicated, may hold values from 0.1 to 1.9
- norm_gain: float32 [2048], replicated, may hold values from 0.1 to 1.9
- route_expert: int32 [4096, 2], P(('sp', 'tp')), may hold values from 0 to 31, all different within a row; in each aligned block of 128 rows (0 to 127, 128 to 255, ...) at most 16 rows name the same one
- route_weight: float32 [4096, 2], P(('sp', 'tp')), may hold values from 0.2 to 1
- expert_gate: bfloat16 [32, 2048, 1024], P(('sp', 'tp')), may hold values from -0.125 to 0.125
- expert_up: bfloat16 [32, 2048, 1024], P(('sp', 'tp')), may hold values from -0.125 to 0.125
- expert_down: bfloat16 [32, 1024, 2048], P(('sp', 'tp')), may hold values from -0.1875 to 0.1875
Outputs:
- output: bfloat16 [4096, 2048], P(('sp', 'tp'))
Inputs may be any that keep to these rules, and one draw needn't show every extreme that they name: `route_expert`: each row names 2 different experts. The rows of one device (aligned blocks of 128 rows) name any one expert at most 16 times, and in some blocks some expert is named exactly 16 times.
All inputs are finite; a program needn't handle non-finite values.
Results may differ from a plain program's by a relative error of at most 0.015.
Values may be sent and summed in bfloat16 or wider, within the bound.
A program may use at most 128 MiB of HBM per device.

v0:
```python
import math

import jax
import jax.numpy as jnp
from jax import lax
from jax.sharding import PartitionSpec as P

D = 2048
HEAD_SIZE = 64
GRID_W = 64


epsilon = 1e-06
base_theta = 10000.0


def unit_length_rows(values):
    values = values.astype(jnp.float32)
    return values * lax.rsqrt(jnp.mean(values * values, axis=-1, keepdims=True) + epsilon)


def rotary_embed(head_vecs, offset):
    row_count = head_vecs.shape[0]
    quarter = head_vecs.shape[-1] // 4
    places = offset + jnp.arange(row_count, dtype=jnp.int32)
    grid_row = (places // GRID_W).astype(jnp.float32)
    grid_col = (places % GRID_W).astype(jnp.float32)
    frequency = base_theta ** (-jnp.arange(quarter, dtype=jnp.float32) / quarter)
    row_angle = grid_row[:, None, None] * frequency
    col_angle = grid_col[:, None, None] * frequency
    row_cos, row_sin = (jnp.cos(row_angle), jnp.sin(row_angle))
    col_cos, col_sin = (jnp.cos(col_angle), jnp.sin(col_angle))
    row_first = head_vecs[..., :quarter]
    row_second = head_vecs[..., quarter : 2 * quarter]
    col_first = head_vecs[..., 2 * quarter : 3 * quarter]
    col_second = head_vecs[..., 3 * quarter :]
    return jnp.concatenate(
        [
            row_first * row_cos - row_second * row_sin,
            row_second * row_cos + row_first * row_sin,
            col_first * col_cos - col_second * col_sin,
            col_second * col_cos + col_first * col_sin,
        ],
        axis=-1,
    )


def local(
    query_proj,
    projected_keys,
    projected_values,
    residual,
    out_weight,
    mix_gain,
    norm_gain,
    route_expert,
    route_weight,
    expert_gate,
    expert_up,
    expert_down,
):
    tok_count = query_proj.shape[0]
    q_heads = query_proj.shape[1] // HEAD_SIZE
    kv_heads = projected_keys.shape[1] // HEAD_SIZE
    query_group = q_heads // kv_heads
    offset = lax.axis_index("sp") * tok_count
    query_prepared = rotary_embed(
        unit_length_rows(query_proj.reshape(tok_count, q_heads, HEAD_SIZE)), offset
    ).astype(jnp.bfloat16)
    query_prepared = query_prepared.reshape(tok_count, kv_heads, query_group, HEAD_SIZE)
    key_prepared = rotary_embed(
        unit_length_rows(projected_keys.reshape(tok_count, kv_heads, HEAD_SIZE)), offset
    ).astype(jnp.bfloat16)
    v_ready = projected_values.reshape(tok_count, kv_heads, HEAD_SIZE)
    scale = HEAD_SIZE ** (-0.5)
    sums_start = jnp.zeros((tok_count, kv_heads, query_group, HEAD_SIZE), jnp.float32)
    totals_start = jnp.zeros((tok_count, kv_heads, query_group), jnp.float32)
    keys_all = lax.all_gather(key_prepared, "sp", axis=0, tiled=True)
    vals_all = lax.all_gather(v_ready, "sp", axis=0, tiled=True)
    key_count = keys_all.shape[0]
    model_width = math.gcd(key_count, 1024)
    key_blocks = keys_all.reshape(key_count // model_width, model_width, kv_heads, HEAD_SIZE)
    val_blocks = vals_all.reshape(key_count // model_width, model_width, kv_heads, HEAD_SIZE)

    def one_block(inner, pair):
        sums, totals = inner
        scores = (
            jnp.einsum(
                "thgd,nhd->thgn", query_prepared, pair[0], preferred_element_type=jnp.float32
            )
            * scale
        )
        weights = jnp.exp(scores)
        totals = totals + jnp.sum(weights, axis=-1)
        sums = sums + jnp.einsum(
            "thgn,nhd->thgd",
            weights.astype(jnp.bfloat16),
            pair[1],
            preferred_element_type=jnp.float32,
        )
        return ((sums, totals), None)

    result, unused = lax.scan(one_block, (sums_start, totals_start), (key_blocks, val_blocks))
    sums, totals = result
    attended = (
        (sums / totals[..., None]).astype(jnp.bfloat16).reshape(tok_count, q_heads * HEAD_SIZE)
    )
    by_token = lax.all_to_all(attended, "tp", split_axis=0, concat_axis=1, tiled=True)
    mixed = jnp.dot(by_token, out_weight, preferred_element_type=jnp.float32)
    stream = (residual.astype(jnp.float32) + unit_length_rows(mixed) * mix_gain).astype(
        jnp.bfloat16
    )
    normed = (unit_length_rows(stream) * norm_gain).astype(jnp.bfloat16)
    row_count = normed.shape[0]
    top_count = route_expert.shape[1]
    experts = lax.axis_size("sp") * lax.axis_size("tp")
    capacity = max(2, 2 * top_count * row_count // experts)
    flat_expert = route_expert.reshape(-1)
    onehot = (flat_expert[:, None] == jnp.arange(experts, dtype=jnp.int32)[None, :]).astype(
        jnp.int32
    )
    earlier = jnp.cumsum(onehot, axis=0) - onehot
    slot_rank = jnp.sum(earlier * onehot, axis=1)
    target = flat_expert * capacity + slot_rank
    placing = jnp.arange(experts * capacity, dtype=jnp.int32)[:, None] == target[None, :]
    placing = jnp.any(placing.reshape(experts * capacity, row_count, top_count), axis=2).astype(
        jnp.bfloat16
    )
    outgoing = jnp.dot(placing, normed, preferred_element_type=jnp.float32).astype(jnp.bfloat16)
    outgoing = outgoing.reshape(experts, capacity, D)
    gate_mat = expert_gate[0]
    up_mat = expert_up[0]
    down_mat = expert_down[0]
    slots = lax.all_to_all(outgoing, ("sp", "tp"), split_axis=0, concat_axis=0, tiled=True)
    flat_rows = slots.reshape(-1, slots.shape[-1])
    gate_pre = jnp.dot(flat_rows, gate_mat, preferred_element_type=jnp.float32)
    up_pre = jnp.dot(flat_rows, up_mat, preferred_element_type=jnp.float32)
    expert_act = (jax.nn.silu(gate_pre) * up_pre).astype(jnp.bfloat16)
    done = jnp.dot(expert_act, down_mat, preferred_element_type=jnp.float32).astype(jnp.bfloat16)
    answered = done.reshape(slots.shape)
    returned = lax.all_to_all(answered, ("sp", "tp"), split_axis=0, concat_axis=0, tiled=True)
    picked = jnp.take(returned.reshape(experts * capacity, D), target, axis=0).reshape(
        row_count, top_count, D
    )
    combined = jnp.sum(picked.astype(jnp.float32) * route_weight[:, :, None], axis=1)
    return (stream.astype(jnp.float32) + combined).astype(jnp.bfloat16)


def solution(mesh):
    return jax.shard_map(
        local,
        mesh=mesh,
        in_specs=(
            P("sp", "tp"),
            P("sp", "tp"),
            P("sp", "tp"),
            P(("sp", "tp"), None),
            P(),
            P(),
            P(),
            P(("sp", "tp"), None),
            P(("sp", "tp"), None),
            P(("sp", "tp"), None, None),
            P(("sp", "tp"), None, None),
            P(("sp", "tp"), None, None),
        ),
        out_specs=P(("sp", "tp"), None),
        check_vma=False,
    )
```

profile of v0, /device:TPU:16, one launch (start us, length us, event | category | flops | bytes accessed | tf_op | source)
XLA Modules:
  0.0 275.1 jit_solution(4073406177149737743)
XLA Ops:
  8.8 1.7 copy.71
  14.1 34.6 %all-gather.5.cloned.1.call-done = bf16[4096,2,64]{0,2,1:T(8,128)(2,1)} async-done(((bf16[512,2,64]{0,2,1:T(8,128)(2,1)}), bf16[4096,2,64]{0,2,1:T(8,128)(2,1)}) %all-gather.5.cloned.1.call-update) | async-done | bytes 1048592 | tf_op jit(solution)/shard_map/all_gather | solution.py:78
  48.7 1.3 copy.93
  50.0 39.2 %all-gather.3.cloned.1.call-done = bf16[4096,2,64]{0,2,1:T(8,128)(2,1)} async-done(((bf16[512,2,64]{0,2,1:T(8,128)(2,1)}), bf16[4096,2,64]{0,2,1:T(8,128)(2,1)}) %all-gather.3.cloned.1.call-update) | async-done | bytes 1048592 | tf_op jit(solution)/shard_map/all_gather | solution.py:79
  90.5 38.0 %while.13 = (s32[]{:T(128)}, f32[512,2,2,64]{0,3,2,1:T(8,128)S(1)}, f32[512,2,2]{0,2,1:T(2,128)S(1)}, bf16[4,1024,2,64]{1,3,2,0:T(8,128)(2,1)S(1)}, bf16[4,1024,...) while((s32[]{:T(128)}, f32[512,2,2,64]{0,3,2,1:T(8,128)S(1)}, ...), condition=%wide.region_4.5_spmd.clone, body=%wide.region_2.4_spmd.clone.sunk | while | flops 545523712 | bytes 18645096 | solution.py:103
  90.6 4.6 %bitcast_reduce_fusion.2 = (f32[512,2,2]{0,2,1:T(2,128)S(1)}, f32[2,1024,512,2]{2,1,3,0:T(8,128)}) fusion(bf16[512,2,2,64]{0,3,2,1:T(8,128)(2,1)S(1)} %get-tuple-element.193, bf16[4,1024,2,64]{1,3,2,0:T(8,128)(2,1)S(1)} %get-tuple-element.192, s32[]{:T(128)} %get-tuple-element.180), kind=kOutput, calls=%fused_computation.1.clone.1 | convolution fusion | flops 272627712 | bytes 8921092 | tf_op jit(solution)/shard_map/while/body/eval_jaxpr/thgd,nhd->thgn/dot_general | solution.py:88
  95.2 4.9 %fusion.58 = f32[512,2,2,64]{0,3,2,1:T(8,128)S(1)} fusion(f32[2,1024,512,2]{2,1,3,0:T(8,128)} %get-tuple-element.170, f32[512,2,2,64]{0,3,2,1:T(8,128)S(1)} %get-tuple-element.181, bf16[4,1024,2,64]{1,3,2,0:T(8,128)(2,1)S(1)} %get-tuple-element.191, s32[]{:T(128)} %get-tuple-element.180, pred[]{:T(512)S(6)} %compare.14), kind=kOutput, calls=%fused_computation.7.clone.1 | convolution fusion | flops 272891904 | bytes 9699333 | tf_op jit(solution)/shard_map/while/body/eval_jaxpr/thgn,nhd->thgd/dot_general | solution.py:95
  100.1 4.6 %bitcast_reduce_fusion.2 = (f32[512,2,2]{0,2,1:T(2,128)S(1)}, f32[2,1024,512,2]{2,1,3,0:T(8,128)}) fusion(bf16[512,2,2,64]{0,3,2,1:T(8,128)(2,1)S(1)} %get-tuple-element.193, bf16[4,1024,2,64]{1,3,2,0:T(8,128)(2,1)S(1)} %get-tuple-element.192, s32[]{:T(128)} %get-tuple-element.180), kind=kOutput, calls=%fused_computation.1.clone.1 | convolution fusion | flops 272627712 | bytes 8921092 | tf_op jit(solution)/shard_map/while/body/eval_jaxpr/thgd,nhd->thgn/dot_general | solution.py:88
  104.7 4.9 %fusion.58 = f32[512,2,2,64]{0,3,2,1:T(8,128)S(1)} fusion(f32[2,1024,512,2]{2,1,3,0:T(8,128)} %get-tuple-element.170, f32[512,2,2,64]{0,3,2,1:T(8,128)S(1)} %get-tuple-element.181, bf16[4,1024,2,64]{1,3,2,0:T(8,128)(2,1)S(1)} %get-tuple-element.191, s32[]{:T(128)} %get-tuple-element.180, pred[]{:T(512)S(6)} %compare.14), kind=kOutput, calls=%fused_computation.7.clone.1 | convolution fusion | flops 272891904 | bytes 9699333 | tf_op jit(solution)/shard_map/while/body/eval_jaxpr/thgn,nhd->thgd/dot_general | solution.py:95
  109.6 4.6 %bitcast_reduce_fusion.2 = (f32[512,2,2]{0,2,1:T(2,128)S(1)}, f32[2,1024,512,2]{2,1,3,0:T(8,128)}) fusion(bf16[512,2,2,64]{0,3,2,1:T(8,128)(2,1)S(1)} %get-tuple-element.193, bf16[4,1024,2,64]{1,3,2,0:T(8,128)(2,1)S(1)} %get-tuple-element.192, s32[]{:T(128)} %get-tuple-element.180), kind=kOutput, calls=%fused_computation.1.clone.1 | convolution fusion | flops 272627712 | bytes 8921092 | tf_op jit(solution)/shard_map/while/body/eval_jaxpr/thgd,nhd->thgn/dot_general | solution.py:88
  114.2 4.9 %fusion.58 = f32[512,2,2,64]{0,3,2,1:T(8,128)S(1)} fusion(f32[2,1024,512,2]{2,1,3,0:T(8,128)} %get-tuple-element.170, f32[512,2,2,64]{0,3,2,1:T(8,128)S(1)} %get-tuple-element.181, bf16[4,1024,2,64]{1,3,2,0:T(8,128)(2,1)S(1)} %get-tuple-element.191, s32[]{:T(128)} %get-tuple-element.180, pred[]{:T(512)S(6)} %compare.14), kind=kOutput, calls=%fused_computation.7.clone.1 | convolution fusion | flops 272891904 | bytes 9699333 | tf_op jit(solution)/shard_map/while/body/eval_jaxpr/thgn,nhd->thgd/dot_general | solution.py:95
  119.1 4.6 %bitcast_reduce_fusion.2 = (f32[512,2,2]{0,2,1:T(2,128)S(1)}, f32[2,1024,512,2]{2,1,3,0:T(8,128)}) fusion(bf16[512,2,2,64]{0,3,2,1:T(8,128)(2,1)S(1)} %get-tuple-element.193, bf16[4,1024,2,64]{1,3,2,0:T(8,128)(2,1)S(1)} %get-tuple-element.192, s32[]{:T(128)} %get-tuple-element.180), kind=kOutput, calls=%fused_computation.1.clone.1 | convolution fusion | flops 272627712 | bytes 8921092 | tf_op jit(solution)/shard_map/while/body/eval_jaxpr/thgd,nhd->thgn/dot_general | solution.py:88
  123.7 4.9 %fusion.58 = f32[512,2,2,64]{0,3,2,1:T(8,128)S(1)} fusion(f32[2,1024,512,2]{2,1,3,0:T(8,128)} %get-tuple-element.170, f32[512,2,2,64]{0,3,2,1:T(8,128)S(1)} %get-tuple-element.181, bf16[4,1024,2,64]{1,3,2,0:T(8,128)(2,1)S(1)} %get-tuple-element.191, s32[]{:T(128)} %get-tuple-element.180, pred[]{:T(512)S(6)} %compare.14), kind=kOutput, calls=%fused_computation.7.clone.1 | convolution fusion | flops 272891904 | bytes 9699333 | tf_op jit(solution)/shard_map/while/body/eval_jaxpr/thgn,nhd->thgd/dot_general | solution.py:95
  129.5 3.5 %all-to-all-start = ((bf16[4,128,256]{1,2,0:T(8,128)(2,1)}), bf16[4,128,256]{1,2,0:T(8,128)(2,1)S(1)}, u32[]{:S(2)}, u32[]{:S(2)}) async-start(bf16[4,128,256]{1,2,0:T(8,128)(2,1)} %copy.76), calls=%async_computation | async-start | bytes 524288 | tf_op jit(solution)/shard_map/all_to_all | solution.py:108
  133.1 5.9 %all-to-all-done = bf16[4,128,256]{1,2,0:T(8,128)(2,1)S(1)} async-done(((bf16[4,128,256]{1,2,0:T(8,128)(2,1)}), bf16[4,128,256]{1,2,0:T(8,128)(2,1)S(1)}, u32[]{:S(2)}, u32[]{:S(2)}) %all-to-all-start) | async-done | bytes 262176 | tf_op jit(solution)/shard_map/all_to_all | solution.py:108
  139.0 3.0 %multiply_reduce_fusion.1 = (f32[128]{0:T(128)S(1)}, f32[128,2048]{1,0:T(8,128)S(1)}) fusion(bf16[128,1024]{0,1:T(8,128)(2,1)S(1)} %bitcast.119, bf16[1024,2048]{1,0:T(8,128)(2,1)} %param.18), kind=kOutput, calls=%fused_computation.38 | convolution fusion | flops 537395072 | bytes 5505536 | tf_op jit(solution)/shard_map/dot_general | solution.py:109
  143.2 50.6 %all_to_all.29 = bf16[32,16,2048]{2,1,0:T(8,128)(2,1)S(1)} all-to-all(bf16[32,16,2048]{2,1,0:T(8,128)(2,1)S(1)} %bitcast.113), channel_id=1, replica_groups=mesh['sp'=8,'tp'=4] {'sp','tp'}, dimensions={0} | all-to-all | bytes 4194304 | tf_op jit(solution)/shard_map/all_to_all | solution.py:134
  193.9 3.7 %fusion.16 = f32[512,1024]{1,0:T(8,128)} fusion(bf16[512,2048]{1,0:T(8,128)(2,1)S(1)} %bitcast.117, bf16[1,2048,1024]{2,1,0:T(8,128)(2,1)S(1)} %copy-done.5), kind=kOutput, calls=%fused_computation.21 | convolution fusion | flops 2147483648 | bytes 8388608 | tf_op jit(solution)/shard_map/dot_general | solution.py:136
  197.6 9.9 %fusion.18 = bf16[512,2048]{1,0:T(8,128)(2,1)} fusion(bf16[1,1024,2048]{2,1,0:T(8,128)(2,1)} %param.25, f32[512,1024]{1,0:T(8,128)} %fusion.16, bf16[512,2048]{1,0:T(8,128)(2,1)S(1)} %bitcast.118, bf16[1,2048,1024]{2,1,0:T(8,128)(2,1)} %param.24), kind=kOutput, calls=%fused_computation.23 | convolution fusion | flops 4299161600 | bytes 14680064 | tf_op jit(solution)/shard_map/dot_general | solution.py:139
  207.5 5.6 %all-to-all-start.2 = ((bf16[32,16,2048]{2,1,0:T(8,128)(2,1)}), bf16[32,16,2048]{2,1,0:T(8,128)(2,1)S(1)}, u32[]{:S(2)}, u32[]{:S(2)}) async-start(bf16[32,16,2048]{2,1,0:T(8,128)(2,1)} %bitcast.116), calls=%async_computation.2 | async-start | bytes 4194304 | tf_op jit(solution)/shard_map/all_to_all | solution.py:141
  213.7 45.5 %all-to-all-done.2 = bf16[32,16,2048]{2,1,0:T(8,128)(2,1)S(1)} async-done(((bf16[32,16,2048]{2,1,0:T(8,128)(2,1)}), bf16[32,16,2048]{2,1,0:T(8,128)(2,1)S(1)}, u32[]{:S(2)}, u32[]{:S(2)}) %all-to-all-start.2) | async-done | bytes 2097184 | tf_op jit(solution)/shard_map/all_to_all | solution.py:141
  259.1 2.3 gather_fusion
  261.5 1.7 gather.7
  263.2 4.1 %multiply_reduce_fusion = f32[128,2048]{1,0:T(8,128)S(1)} fusion(bf16[128,2,2048]{2,1,0:T(2,128)(2,1)S(1)} %gather.7, pred[128,2]{1,0:T(8,128)(4,1)S(1)} %copy.81, f32[128,2]{1,0:T(8,128)S(1)} %copy.83), kind=kLoop, calls=%fused_computation.25 | loop fusion | flops 1835008 | bytes 2098432 | tf_op jit(solution)/shard_map/reduce_sum | solution.py:145
  (66 shorter events, 10.7 us)
Async XLA Ops:
  6.5 42.2 %all-gather.5.cloned.1.call-start = ((), (), s32[]{:S(2)}) async-start(), calls=%async_computation.4 | async-start | bytes 1179648 | tf_op jit(solution)/shard_map/all_gather | solution.py:78
  8.7 80.5 %all-gather.3.cloned.1.call-start = ((), (), s32[]{:S(2)}) async-start(), calls=%async_computation.3 | async-start | bytes 1179648 | tf_op jit(solution)/shard_map/all_gather | solution.py:79
  90.5 42.5 %copy-start.1 = (s32[128,2]{0,1:T(2,128)S(1)}, s32[128,2]{0,1:T(2,128)}, u32[]{:S(2)}) copy-start(s32[128,2]{0,1:T(2,128)} %param.21) | copy-start | bytes 3076
  128.6 13.4 %copy-start = (bf16[128,2048]{1,0:T(8,128)(2,1)S(1)}, bf16[128,2048]{1,0:T(8,128)(2,1)}, u32[]{:S(2)}) copy-start(bf16[128,2048]{1,0:T(8,128)(2,1)} %param.17) | copy-start | bytes 1572868
  128.6 13.4 %copy-start.2 = (f32[2048]{0:T(1024)S(1)}, f32[2048]{0:T(1024)}, u32[]{:S(2)}) copy-start(f32[2048]{0:T(1024)} %param.19) | copy-start | bytes 24580
  129.5 13.0 %copy-start.3 = (f32[2048]{0:T(1024)S(1)}, f32[2048]{0:T(1024)}, u32[]{:S(2)}) copy-start(f32[2048]{0:T(1024)} %param.20) | copy-start | bytes 24580
  129.5 9.5 %all-to-all-start = ((bf16[4,128,256]{1,2,0:T(8,128)(2,1)}), bf16[4,128,256]{1,2,0:T(8,128)(2,1)S(1)}, u32[]{:S(2)}, u32[]{:S(2)}) async-start(bf16[4,128,256]{1,2,0:T(8,128)(2,1)} %copy.76), calls=%async_computation | async-start | bytes 524288 | tf_op jit(solution)/shard_map/all_to_all | solution.py:108
  142.0 51.8 %copy-start.5 = (bf16[1,2048,1024]{2,1,0:T(8,128)(2,1)S(1)}, bf16[1,2048,1024]{2,1,0:T(8,128)(2,1)}, u32[]{:S(2)}) copy-start(bf16[1,2048,1024]{2,1,0:T(8,128)(2,1)} %param.23) | copy-start | bytes 12582916
  207.5 6.1 %copy-start.4 = (f32[128,2]{0,1:T(2,128)S(1)}, f32[128,2]{0,1:T(2,128)}, u32[]{:S(2)}) copy-start(f32[128,2]{0,1:T(2,128)} %param.22) | copy-start | bytes 3076
  207.5 51.7 %all-to-all-start.2 = ((bf16[32,16,2048]{2,1,0:T(8,128)(2,1)}), bf16[32,16,2048]{2,1,0:T(8,128)(2,1)S(1)}, u32[]{:S(2)}, u32[]{:S(2)}) async-start(bf16[32,16,2048]{2,1,0:T(8,128)(2,1)} %bitcast.116), calls=%async_computation.2 | async-start | bytes 4194304 | tf_op jit(solution)/shard_map/all_to_all | solution.py:141
Sparse Core Ops, SparseCore 0:
  9.4 39.3 all-gather.4
  50.8 38.3 all-gather.2
where the time goes:
time: 280 us; the launch traced here: 275 us
  waiting for transfers between devices  125 us (45%)
  matrix products  55.3 us (20%)
  blocking collectives  50.6 us (18%)
  between operations  13.7 us (5%)
  local copies, waits for them, and re-layouts  13.3 us (5%)
  starting transfers between devices  9.22 us (3%)
  other arithmetic  7.72 us (3%)
    all_to_all x1, blocking collectives, local(): lax.all_to_all(outgoing, ('sp', 'tp'), split_axis=0, concat_axis=0, tiled...  50.6 us
    all_to_all x1, waiting for transfers between devices, local(): lax.all_to_all(answered, ('sp', 'tp'), split_axis=0, concat_axis=0, tiled...  45.5 us
    all_gather x1, waiting for transfers between devices, local(): vals_all = lax.all_gather(v_ready, 'sp', axis=0, tiled=True)  39.2 us
    all_gather x1, waiting for transfers between devices, local(): keys_all = lax.all_gather(key_prepared, 'sp', axis=0, tiled=True)  34.6 us
    dot_general x4, matrix products, one_block(): jnp.einsum('thgn,nhd->thgd', weights.astype(jnp.bfloat16), pair[1], prefe...  19.4 us
    dot_general x4, matrix products, one_block(): jnp.einsum('thgd,nhd->thgn', query_prepared, pair[0], preferred_element_t...  18.4 us
    dot_general x1, matrix products, local(): jnp.dot(expert_act, down_mat, preferred_element_type=jnp.float32)  9.9 us
    all_to_all x1, waiting for transfers between devices, local(): lax.all_to_all(attended, 'tp', split_axis=0, concat_axis=1, tiled=True)  5.88 us
  transfers between devices with their start and end apart: 4, of which 4 were waited for; matrix products, arithmetic and copies ran while one was open for 3% of the time, Pallas kernels for 0%

commit v1 on v0

v1 whole, which is shorter than its diff:
```python
import functools
import math

import jax
import jax.numpy as jnp
from jax import lax
from jax.experimental import pallas as pl
from jax.experimental.pallas import tpu as pltpu
from jax.sharding import PartitionSpec as P

D = 2048
HEAD_SIZE = 64
GRID_W = 64


epsilon = 1e-06
base_theta = 10000.0


def unit_length_rows(values):
    values = values.astype(jnp.float32)
    return values * lax.rsqrt(jnp.mean(values * values, axis=-1, keepdims=True) + epsilon)


MESH = pl.DeviceIdType.MESH
LANES = 2 * HEAD_SIZE


def ring_step(sp, delta, n, nz, nx):
    z, x = sp // nx, sp % nx
    place = x * nz + z + (x % 2) * (nz - 1 - 2 * z)
    place = (place + delta + n) % n
    x = place // nz
    z = place % nz
    z = z + (x % 2) * (nz - 1 - 2 * z)
    return z * nx + x


def attend_kernel(
    n, nz, nx, ntp, group,
    q_ref, k_ref, v_ref, cos_ref, sin_ref, swap_ref, ones_ref,
    out_ref,
    qs, acc, fb, bb, att, rx,
    send_f, recv_f, send_b, recv_b, send_t, recv_t,
):
    sp = lax.axis_index("sp")
    tp = lax.axis_index("tp")
    toks = q_ref.shape[0]
    heads = q_ref.shape[1] // HEAD_SIZE
    half = toks // 2
    steps = n - 1
    nxt = ring_step(sp, 1, n, nz, nx)
    prv = ring_step(sp, -1, n, nz, nx)

    barrier = pltpu.get_barrier_semaphore()
    for other in (nxt, prv):
        pl.semaphore_signal(barrier, inc=1, device_id=(other, tp), device_id_type=MESH)
    for d in range(1, ntp):
        pl.semaphore_signal(
            barrier, inc=1, device_id=(sp, (tp + d) % ntp), device_id_type=MESH
        )

    cos = cos_ref[...]
    sin = sin_ref[...]
    low = lax.broadcasted_iota(jnp.int32, (toks, LANES), 1) < HEAD_SIZE

    def prepare(block):
        wide = block.astype(jnp.float32)
        square = wide * wide
        hi = square.astype(jnp.bfloat16)
        lo = (square - hi.astype(jnp.float32)).astype(jnp.bfloat16)
        mean = jnp.dot(hi, ones_ref[...], preferred_element_type=jnp.float32) + jnp.dot(
            lo, ones_ref[...], preferred_element_type=jnp.float32
        )
        partner = jnp.dot(block, swap_ref[...], preferred_element_type=jnp.float32)
        return (wide * cos + partner * sin) * lax.rsqrt(mean + epsilon)

    keys = prepare(k_ref[...]).astype(jnp.bfloat16)
    vals = v_ref[...]
    for c in range(2):
        rows = slice(c * half, (c + 1) * half)
        fb[c, 0] = keys[rows]
        fb[c, 1] = vals[rows]
        bb[1 - c, 0] = keys[rows]
        bb[1 - c, 1] = vals[rows]

    def forward(i):
        return pltpu.make_async_remote_copy(
            src_ref=fb.at[i], dst_ref=fb.at[i + 2],
            send_sem=send_f.at[i], recv_sem=recv_f.at[i],
            device_id=(nxt, tp), device_id_type=MESH,
        )

    def backward(i):
        return pltpu.make_async_remote_copy(
            src_ref=bb.at[i], dst_ref=bb.at[i + 2],
            send_sem=send_b.at[i], recv_sem=recv_b.at[i],
            device_id=(prv, tp), device_id_type=MESH,
        )

    pl.semaphore_wait(barrier, 2 + ntp - 1)
    for i in range(2):
        forward(i).start()
        backward(i).start()

    scale = HEAD_SIZE ** (-0.5)
    for t in range(heads // 2):
        ready = prepare(q_ref[:, t * LANES : (t + 1) * LANES]) * scale
        for h in (2 * t, 2 * t + 1):
            side = (h // group) % 2
            lined = ready if h % 2 == side else pltpu.roll(ready, HEAD_SIZE, 1)
            keep = low if side == 0 else jnp.logical_not(low)
            qs[h * toks : (h + 1) * toks] = jnp.where(keep, lined, 0.0).astype(jnp.bfloat16)
    acc[...] = jnp.zeros_like(acc)
    tile = math.gcd(toks, 256)
    vlow = lax.broadcasted_iota(jnp.int32, (toks, LANES), 1) < HEAD_SIZE

    def one_step(j, carry):
        at = j + jnp.minimum(j, 1)

        @pl.when(j > 0)
        def _():
            forward(j - 1).wait_recv()
            backward(j - 1).wait_recv()

        @pl.when(jnp.logical_and(j > 0, j + 1 < steps))
        def _():
            forward(j + 1).start()
            backward(j + 1).start()

        kk = jnp.concatenate([fb[at, 0], bb[at, 0]], axis=0)
        vv = jnp.concatenate([fb[at, 1], bb[at, 1]], axis=0).astype(jnp.float32)
        sided = (
            jnp.where(vlow, vv, 1.0).astype(jnp.bfloat16),
            jnp.where(vlow, 1.0, vv).astype(jnp.bfloat16),
        )
        for h in range(heads):
            for r in range(toks // tile):
                rows = slice(h * toks + r * tile, h * toks + (r + 1) * tile)
                scores = lax.dot_general(
                    qs[rows], kk, (((1,), (1,)), ((), ())),
                    preferred_element_type=jnp.float32,
                )
                weights = jnp.exp(scores).astype(jnp.bfloat16)
                acc[rows] += jnp.dot(
                    weights, sided[(h // group) % 2], preferred_element_type=jnp.float32
                )
        return carry

    lax.fori_loop(0, steps + 1, one_step, 0)

    share = toks // ntp
    for t in range(heads // 2):
        parts = []
        for h in (2 * t, 2 * t + 1):
            mine = acc[h * toks : (h + 1) * toks]
            turned = pltpu.roll(mine, HEAD_SIZE, 1)
            parts.append(mine / turned if h % 2 == (h // group) % 2 else turned / mine)
        done = jnp.where(low, parts[0], parts[1]).astype(jnp.bfloat16)
        for p in range(ntp):
            att[p, :, t * LANES : (t + 1) * LANES] = done[p * share : (p + 1) * share]

    def across(d):
        to = (tp + d) % ntp
        return pltpu.make_async_remote_copy(
            src_ref=att.at[to], dst_ref=rx.at[tp],
            send_sem=send_t.at[d], recv_sem=recv_t.at[d],
            device_id=(sp, to), device_id_type=MESH,
        )

    for d in range(1, ntp):
        across(d).start()
    rx[tp] = att[tp]
    for i in range(steps):
        forward(i).wait_send()
        backward(i).wait_send()
    for d in range(1, ntp):
        across(d).wait_recv()
    width = q_ref.shape[1]
    for p in range(ntp):
        out_ref[:, p * width : (p + 1) * width] = rx[p]
    for d in range(1, ntp):
        across(d).wait_send()


def ring_sizes(mesh, n):
    try:
        coords = [tuple(d.coords) for d in mesh.devices[:, 0]]
        nz = len({c[2] for c in coords})
        nx = len({c[0] for c in coords})
        if nz * nx == n and nz > 1:
            return nz, nx
    except Exception:
        pass
    return n, 1


def attend(mesh, query_proj, projected_keys, projected_values):
    n, ntp = mesh.shape["sp"], mesh.shape["tp"]
    nz, nx = ring_sizes(mesh, n)
    toks, width = query_proj.shape
    heads = width // HEAD_SIZE
    group = heads // (projected_keys.shape[1] // HEAD_SIZE)
    spare = LANES - projected_keys.shape[1]
    if spare:
        projected_keys = jnp.pad(projected_keys, ((0, 0), (0, spare)))
        projected_values = jnp.pad(projected_values, ((0, 0), (0, spare)))
    quarter = HEAD_SIZE // 4
    places = lax.axis_index("sp") * toks + jnp.arange(toks, dtype=jnp.int32)
    frequency = base_theta ** (-jnp.arange(quarter, dtype=jnp.float32) / quarter)
    lane = jnp.arange(LANES, dtype=jnp.int32)
    on_row = (lane % HEAD_SIZE) < 2 * quarter
    spot = jnp.where(on_row[None, :], (places // GRID_W)[:, None], (places % GRID_W)[:, None])
    angle = spot.astype(jnp.float32) * jnp.tile(frequency, LANES // quarter)[None, :]
    first = (lane // quarter) % 2 == 0
    source = jnp.where(first, lane + quarter, lane - quarter)
    swap = jnp.where(
        lane[:, None] == source[None, :], jnp.where(first, -1.0, 1.0)[None, :], 0.0
    ).astype(jnp.bfloat16)
    ones = jnp.where(
        lane[:, None] // HEAD_SIZE == lane[None, :] // HEAD_SIZE, 1.0 / HEAD_SIZE, 0.0
    ).astype(jnp.bfloat16)
    share = toks // ntp
    dma = pltpu.SemaphoreType.DMA
    return pl.pallas_call(
        functools.partial(attend_kernel, n, nz, nx, ntp, group),
        out_shape=jax.ShapeDtypeStruct((share, ntp * width), jnp.bfloat16),
        in_specs=[pl.BlockSpec(memory_space=pltpu.VMEM)] * 7,
        out_specs=pl.BlockSpec(memory_space=pltpu.VMEM),
        scratch_shapes=[
            pltpu.VMEM((heads * toks, LANES), jnp.bfloat16),
            pltpu.VMEM((heads * toks, LANES), jnp.float32),
            pltpu.VMEM((n + 1, 2, toks // 2, LANES), jnp.bfloat16),
            pltpu.VMEM((n + 1, 2, toks // 2, LANES), jnp.bfloat16),
            pltpu.VMEM((ntp, share, width), jnp.bfloat16),
            pltpu.VMEM((ntp, share, width), jnp.bfloat16),
            dma((n - 1,)), dma((n - 1,)), dma((n - 1,)), dma((n - 1,)),
            dma((ntp,)), dma((ntp,)),
        ],
        compiler_params=pltpu.CompilerParams(
            collective_id=0, has_side_effects=True, vmem_limit_bytes=40 << 20
        ),
        name="attend",
    )(query_proj, projected_keys, projected_values, jnp.cos(angle), jnp.sin(angle), swap, ones)


def local(
    mesh,
    query_proj,
    projected_keys,
    projected_values,
    residual,
    out_weight,
    mix_gain,
    norm_gain,
    route_expert,
    route_weight,
    expert_gate,
    expert_up,
    expert_down,
):
    by_token = attend(mesh, query_proj, projected_keys, projected_values)
    mixed = jnp.dot(by_token, out_weight, preferred_element_type=jnp.float32)
    stream = (residual.astype(jnp.float32) + unit_length_rows(mixed) * mix_gain).astype(
        jnp.bfloat16
    )
    normed = (unit_length_rows(stream) * norm_gain).astype(jnp.bfloat16)
    row_count = normed.shape[0]
    top_count = route_expert.shape[1]
    experts = lax.axis_size("sp") * lax.axis_size("tp")
    capacity = max(2, 2 * top_count * row_count // experts)
    flat_expert = route_expert.reshape(-1)
    onehot = (flat_expert[:, None] == jnp.arange(experts, dtype=jnp.int32)[None, :]).astype(
        jnp.int32
    )
    earlier = jnp.cumsum(onehot, axis=0) - onehot
    slot_rank = jnp.sum(earlier * onehot, axis=1)
    target = flat_expert * capacity + slot_rank
    placing = jnp.arange(experts * capacity, dtype=jnp.int32)[:, None] == target[None, :]
    placing = jnp.any(placing.reshape(experts * capacity, row_count, top_count), axis=2).astype(
        jnp.bfloat16
    )
    outgoing = jnp.dot(placing, normed, preferred_element_type=jnp.float32).astype(jnp.bfloat16)
    outgoing = outgoing.reshape(experts, capacity, D)
    gate_mat = expert_gate[0]
    up_mat = expert_up[0]
    down_mat = expert_down[0]
    slots = lax.all_to_all(outgoing, ("sp", "tp"), split_axis=0, concat_axis=0, tiled=True)
    flat_rows = slots.reshape(-1, slots.shape[-1])
    gate_pre = jnp.dot(flat_rows, gate_mat, preferred_element_type=jnp.float32)
    up_pre = jnp.dot(flat_rows, up_mat, preferred_element_type=jnp.float32)
    expert_act = (jax.nn.silu(gate_pre) * up_pre).astype(jnp.bfloat16)
    done = jnp.dot(expert_act, down_mat, preferred_element_type=jnp.float32).astype(jnp.bfloat16)
    answered = done.reshape(slots.shape)
    returned = lax.all_to_all(answered, ("sp", "tp"), split_axis=0, concat_axis=0, tiled=True)
    picked = jnp.take(returned.reshape(experts * capacity, D), target, axis=0).reshape(
        row_count, top_count, D
    )
    combined = jnp.sum(picked.astype(jnp.float32) * route_weight[:, :, None], axis=1)
    return (stream.astype(jnp.float32) + combined).astype(jnp.bfloat16)


def solution(mesh):
    return jax.shard_map(
        functools.partial(local, mesh),
        mesh=mesh,
        in_specs=(
            P("sp", "tp"),
            P("sp", "tp"),
            P("sp", "tp"),
            P(("sp", "tp"), None),
            P(),
            P(),
            P(),
            P(("sp", "tp"), None),
            P(("sp", "tp"), None),
            P(("sp", "tp"), None, None),
            P(("sp", "tp"), None, None),
            P(("sp", "tp"), None, None),
        ),
        out_specs=P(("sp", "tp"), None),
        check_vma=False,
    )
```

time: 280 us -> 170 us (0.61)
  the two profiles are of different devices: /device:TPU:16 before, /device:TPU:0 now
where the time goes in v1:
time: 170 us
  blocking collectives  52.7 us (31%)
  waiting for transfers between devices  48 us (28%)
  Pallas kernels  31.6 us (19%)
  matrix products  17.5 us (10%)
  local copies, waits for them, and re-layouts  8.92 us (5%)
  other arithmetic  7.35 us (4%)
  starting transfers between devices  3.84 us (2%)
    all_to_all x1, blocking collectives, local(): lax.all_to_all(outgoing, ('sp', 'tp'), split_axis=0, concat_axis=0, tiled...  52.7 us
    all_to_all x1, waiting for transfers between devices, local(): lax.all_to_all(answered, ('sp', 'tp'), split_axis=0, concat_axis=0, tiled...  48 us
    pallas_call x1, Pallas kernels, attend(): pl.pallas_call(functools.partial(attend_kernel, n, nz, nx, ntp, group), o...  31.6 us
    dot_general x1, matrix products, local(): jnp.dot(expert_act, down_mat, preferred_element_type=jnp.float32)  9.94 us
    gather x2, local copies, waits for them, and re-layouts, local(): jnp.take(returned.reshape(experts * capacity, D), target, axis=0)  4.09 us
    reduce_sum x1, other arithmetic, local(): jnp.sum(picked.astype(jnp.float32) * route_weight[:, :, None], axis=1)  4.07 us
    all_to_all x1, starting transfers between devices, local(): lax.all_to_all(answered, ('sp', 'tp'), split_axis=0, concat_axis=0, tiled...  3.84 us
    dot_general x1, matrix products, local(): gate_pre = jnp.dot(flat_rows, gate_mat, preferred_element_type=jnp.float32)  3.73 us
  transfers between devices with their start and end apart: 1, of which 1 were waited for; matrix products, arithmetic and copies ran while one was open for 0% of the time, Pallas kernels for 0%

profile of v1, /device:TPU:0, one launch (start us, length us, event | category | flops | bytes accessed | tf_op | source)
XLA Modules:
  0.0 170.1 jit_solution(776758764018546702)
XLA Ops:
  0.1 0.8 copy.27
  1.0 0.1 reshape.264
  1.3 1.0 fusion.21
  2.4 0.9 copy-done
  3.3 0.9 copy-done.1
  4.2 0.9 copy-done.2
  5.1 31.6 %attend.1 = bf16[128,1024]{1,0:T(8,128)(2,1)S(1)} custom-call(bf16[512,256]{1,0:T(8,128)(2,1)S(1)} %copy-done, bf16[512,128]{1,0:T(8,128)(2,1)S(1)} %copy-done.1, bf16[512,128]{1,0:T(8,128)(2,1)S(1)} %copy-done.2, f32[512,128]{1,0:T(8,128)S(1)} %get-tuple-element.10.cos_ref, f32[512,128]{1,0:T(8,128)S(1)} %get-tuple-element.9.sin_ref, ...), custom_call_target="tpu_custom_call" | custom-call | tf_op jit(solution)/shard_map/attend/pallas_call | solution.py:225
  36.7 3.0 %multiply_reduce_fusion.1 = (f32[128]{0:T(128)S(1)}, f32[128,2048]{1,0:T(8,128)S(1)}) fusion(bf16[128,1024]{1,0:T(8,128)(2,1)S(1)} %attend.1, bf16[1024,2048]{1,0:T(8,128)(2,1)} %param.16), kind=kOutput, calls=%fused_computation.20 | convolution fusion | flops 537395072 | bytes 5505536 | tf_op jit(solution)/shard_map/dot_general | solution.py:263
  39.8 0.4 fusion.11
  40.2 0.6 reduce-window.6
  40.8 0.2 slice_reduce_fusion
  41.2 0.1 reduce_sum.42
  41.5 0.8 convolution_convert_fusion
  42.3 52.7 %all_to_all.10 = bf16[32,16,2048]{2,1,0:T(8,128)(2,1)S(1)} all-to-all(bf16[32,16,2048]{2,1,0:T(8,128)(2,1)S(1)} %bitcast.46), channel_id=1, replica_groups=mesh['sp'=8,'tp'=4] {'sp','tp'}, dimensions={0} | all-to-all | bytes 4194304 | tf_op jit(solution)/shard_map/all_to_all | solution.py:288
  95.0 3.7 %fusion.4 = f32[512,1024]{1,0:T(8,128)} fusion(bf16[512,2048]{1,0:T(8,128)(2,1)S(1)} %bitcast.48, bf16[1,2048,1024]{2,1,0:T(8,128)(2,1)S(1)} %copy-done.8), kind=kOutput, calls=%fused_computation.5 | convolution fusion | flops 2147483648 | bytes 8388608 | tf_op jit(solution)/shard_map/dot_general | solution.py:290
  98.7 9.9 %fusion.6 = bf16[512,2048]{1,0:T(8,128)(2,1)} fusion(bf16[1,1024,2048]{2,1,0:T(8,128)(2,1)} %param.23, f32[512,1024]{1,0:T(8,128)} %fusion.4, bf16[512,2048]{1,0:T(8,128)(2,1)S(1)} %bitcast.49, bf16[1,2048,1024]{2,1,0:T(8,128)(2,1)} %param.22), kind=kOutput, calls=%fused_computation.7 | convolution fusion | flops 4299161600 | bytes 14680064 | tf_op jit(solution)/shard_map/dot_general | solution.py:293
  108.6 3.8 %all-to-all-start.1 = ((bf16[32,16,2048]{2,1,0:T(8,128)(2,1)}), bf16[32,16,2048]{2,1,0:T(8,128)(2,1)S(1)}, u32[]{:S(2)}, u32[]{:S(2)}) async-start(bf16[32,16,2048]{2,1,0:T(8,128)(2,1)} %bitcast.47), calls=%async_computation.1 | async-start | bytes 4194304 | tf_op jit(solution)/shard_map/all_to_all | solution.py:295
  112.6 0.1 mul.111
  112.7 0.1 copy.31
  113.0 48.0 %all-to-all-done.1 = bf16[32,16,2048]{2,1,0:T(8,128)(2,1)S(1)} async-done(((bf16[32,16,2048]{2,1,0:T(8,128)(2,1)}), bf16[32,16,2048]{2,1,0:T(8,128)(2,1)S(1)}, u32[]{:S(2)}, u32[]{:S(2)}) %all-to-all-start.1) | async-done | bytes 2097184 | tf_op jit(solution)/shard_map/all_to_all | solution.py:295
  161.0 2.3 %gather_fusion = bf16[256,2048]{1,0:T(8,128)(2,1)} fusion(bf16[512,2048]{1,0:T(8,128)(2,1)S(1)} %bitcast.45, s32[1024]{0:T(1024)S(1)} %pad_clamp_fusion), kind=kCustom, calls=%fused_computation | custom fusion | bytes 2098176 | tf_op jit(solution)/shard_map/jit(_take)/gather | solution.py:296
  163.4 1.7 %gather.7 = bf16[128,2,2048]{2,1,0:T(2,128)(2,1)S(1)} reshape(bf16[256,2048]{1,0:T(8,128)(2,1)} %gather_fusion) | data formatting | bytes 2097152 | tf_op jit(solution)/shard_map/jit(_take)/gather | solution.py:296
  165.1 4.1 %multiply_reduce_fusion = f32[128,2048]{1,0:T(8,128)S(1)} fusion(bf16[128,2,2048]{2,1,0:T(2,128)(2,1)S(1)} %gather.7, pred[128,2]{1,0:T(8,128)(4,1)S(1)} %copy.31, f32[128,2]{1,0:T(8,128)S(1)} %copy.33), kind=kLoop, calls=%fused_computation.9 | loop fusion | flops 1835008 | bytes 2098432 | tf_op jit(solution)/shard_map/reduce_sum | solution.py:299
  169.2 0.9 fusion.14
  (40 shorter events, 0.9 us)
Async XLA Ops:
  2.4 1.0 copy-start
  3.3 0.9 copy-start.1
  4.2 0.9 copy-start.2
  36.7 3.1 %copy-start.3 = (bf16[128,2048]{1,0:T(8,128)(2,1)S(1)}, bf16[128,2048]{1,0:T(8,128)(2,1)}, u32[]{:S(2)}) copy-start(bf16[128,2048]{1,0:T(8,128)(2,1)} %param.15) | copy-start | bytes 1572868
  36.7 3.1 %copy-start.5 = (f32[2048]{0:T(1024)S(1)}, f32[2048]{0:T(1024)}, u32[]{:S(2)}) copy-start(f32[2048]{0:T(1024)} %param.17) | copy-start | bytes 24580
  39.8 1.6 copy-start.4
  39.8 1.7 copy-start.6
  42.3 52.7 %copy-start.8 = (bf16[1,2048,1024]{2,1,0:T(8,128)(2,1)S(1)}, bf16[1,2048,1024]{2,1,0:T(8,128)(2,1)}, u32[]{:S(2)}) copy-start(bf16[1,2048,1024]{2,1,0:T(8,128)(2,1)} %param.21) | copy-start | bytes 12582916
  108.6 4.3 %copy-start.7 = (f32[128,2]{0,1:T(2,128)S(1)}, f32[128,2]{0,1:T(2,128)}, u32[]{:S(2)}) copy-start(f32[128,2]{0,1:T(2,128)} %param.20) | copy-start | bytes 3076
  108.6 52.4 %all-to-all-start.1 = ((bf16[32,16,2048]{2,1,0:T(8,128)(2,1)}), bf16[32,16,2048]{2,1,0:T(8,128)(2,1)S(1)}, u32[]{:S(2)}, u32[]{:S(2)}) async-start(bf16[32,16,2048]{2,1,0:T(8,128)(2,1)} %bitcast.47), calls=%async_computation.1 | async-start | bytes 4194304 | tf_op jit(solution)/shard_map/all_to_all | solution.py:295

commit v2 on v1

--- a/solution.py
+++ b/solution.py
@@ -244,6 +244,137 @@
     )(query_proj, projected_keys, projected_values, jnp.cos(angle), jnp.sin(angle), swap, ones)
 
 
+def moe_kernel(
+    count, ntp, cap,
+    tx, stream, pick, share_w, gate_hbm, up_hbm, down_hbm,
+    out_ref,
+    rx, res, ret, act, gate, up, down,
+    send_o, recv_o, send_r, recv_r, wsem,
+):
+    me = lax.axis_index("sp") * ntp + lax.axis_index("tp")
+    per = count // 4
+    order = (2, 1, 3, 0)
+
+    def device(offset):
+        other = (me + offset + count) % count
+        return (other // ntp, other % ntp)
+
+    def block(d):
+        return pl.ds(pl.multiple_of(d * cap, cap), cap)
+
+    def dispatch(d):
+        return pltpu.make_async_remote_copy(
+            src_ref=tx.at[block(d)], dst_ref=rx.at[block(d)],
+            send_sem=send_o.at[d], recv_sem=recv_o.at[d],
+            device_id=device(d), device_id_type=MESH,
+        )
+
+    def answer(d):
+        return pltpu.make_async_remote_copy(
+            src_ref=res.at[block(d)], dst_ref=ret.at[block(d)],
+            send_sem=send_r.at[d], recv_sem=recv_r.at[d],
+            device_id=device(-d), device_id_type=MESH,
+        )
+
+    def each(first, last, action):
+        def body(d, carry):
+            action(d)
+            return carry
+
+        lax.fori_loop(max(first, 1), last, body, 0)
+
+    barrier = pltpu.get_barrier_semaphore()
+    each(1, count, lambda d: pl.semaphore_signal(
+        barrier, inc=1, device_id=device(d), device_id_type=MESH
+    ))
+    loads = [
+        pltpu.make_async_copy(gate_hbm.at[0], gate, wsem.at[0]),
+        pltpu.make_async_copy(up_hbm.at[0], up, wsem.at[1]),
+        pltpu.make_async_copy(down_hbm.at[0], down, wsem.at[2]),
+    ]
+    pl.semaphore_wait(barrier, count - 1)
+    for g in order:
+        each(g * per, (g + 1) * per, lambda d: dispatch(d).start())
+    for load in loads:
+        load.start()
+    rx[0:cap] = tx[0:cap]
+
+    def columns(total, body):
+        tile = math.gcd(total, 256)
+
+        def one(c, carry):
+            body(pl.ds(pl.multiple_of(c * tile, tile), tile))
+            return carry
+
+        lax.fori_loop(0, total // tile, one, 0)
+
+    for number, g in enumerate(order):
+        each(g * per, (g + 1) * per, lambda d: dispatch(d).wait_recv())
+        if number == 0:
+            for load in loads:
+                load.wait()
+        rows = slice(g * per * cap, (g + 1) * per * cap)
+
+        def hidden(cols):
+            taken = rx[rows]
+            pre = jnp.dot(taken, gate[:, cols], preferred_element_type=jnp.float32)
+            lift = jnp.dot(taken, up[:, cols], preferred_element_type=jnp.float32)
+            act[:, cols] = (pre / (1.0 + jnp.exp(-pre)) * lift).astype(jnp.bfloat16)
+
+        def project(cols):
+            res[rows, cols] = jnp.dot(
+                act[...], down[:, cols], preferred_element_type=jnp.float32
+            ).astype(jnp.bfloat16)
+
+        columns(gate.shape[1], hidden)
+        columns(down.shape[1], project)
+        each(g * per, (g + 1) * per, lambda d: answer(d).start())
+    ret[0:cap] = res[0:cap]
+    each(1, count, lambda d: answer(d).wait_recv())
+
+    def combine(cols):
+        total = jnp.zeros((out_ref.shape[0], math.gcd(out_ref.shape[1], 256)), jnp.float32)
+        for k in range(pick.shape[0]):
+            total += share_w[:, k : k + 1] * jnp.dot(
+                pick[k], ret[:, cols], preferred_element_type=jnp.float32
+            )
+        out_ref[:, cols] = (stream[:, cols].astype(jnp.float32) + total).astype(jnp.bfloat16)
+
+    columns(out_ref.shape[1], combine)
+    each(1, count, lambda d: dispatch(d).wait_send())
+    each(1, count, lambda d: answer(d).wait_send())
+
+
+def moe(mesh, cap, outgoing, stream, pick, share_w, expert_gate, expert_up, expert_down):
+    ntp = mesh.shape["tp"]
+    count = mesh.shape["sp"] * ntp
+    width = outgoing.shape[1]
+    ff = expert_gate.shape[2]
+    dma = pltpu.SemaphoreType.DMA
+    low = jnp.bfloat16
+    return pl.pallas_call(
+        functools.partial(moe_kernel, count, ntp, cap),
+        out_shape=jax.ShapeDtypeStruct(stream.shape, low),
+        in_specs=[pl.BlockSpec(memory_space=pltpu.VMEM)] * 4
+        + [pl.BlockSpec(memory_space=pl.ANY)] * 3,
+        out_specs=pl.BlockSpec(memory_space=pltpu.VMEM),
+        scratch_shapes=[
+            pltpu.VMEM((count * cap, width), low),
+            pltpu.VMEM((count * cap, width), low),
+            pltpu.VMEM((count * cap, width), low),
+            pltpu.VMEM((count // 4 * cap, ff), low),
+            pltpu.VMEM((width, ff), low),
+            pltpu.VMEM((width, ff), low),
+            pltpu.VMEM((ff, width), low),
+            dma((count,)), dma((count,)), dma((count,)), dma((count,)), dma((3,)),
+        ],
+        compiler_params=pltpu.CompilerParams(
+            collective_id=1, has_side_effects=True, vmem_limit_bytes=60 << 20
+        ),
+        name="moe",
+    )(outgoing, stream, pick, share_w, expert_gate, expert_up, expert_down)
+
+
 def local(
     mesh,
     query_proj,
@@ -268,36 +399,26 @@
     row_count = normed.shape[0]
     top_count = route_expert.shape[1]
     experts = lax.axis_size("sp") * lax.axis_size("tp")
-    capacity = max(2, 2 * top_count * row_count // experts)
+    capacity = -(-max(2, 2 * top_count * row_count // experts) // 16) * 16
     flat_expert = route_expert.reshape(-1)
     onehot = (flat_expert[:, None] == jnp.arange(experts, dtype=jnp.int32)[None, :]).astype(
         jnp.int32
     )
     earlier = jnp.cumsum(onehot, axis=0) - onehot
     slot_rank = jnp.sum(earlier * onehot, axis=1)
-    target = flat_expert * capacity + slot_rank
+    me = lax.axis_index("sp") * lax.axis_size("tp") + lax.axis_index("tp")
+    target = ((flat_expert - me + experts) % experts) * capacity + slot_rank
     placing = jnp.arange(experts * capacity, dtype=jnp.int32)[:, None] == target[None, :]
     placing = jnp.any(placing.reshape(experts * capacity, row_count, top_count), axis=2).astype(
         jnp.bfloat16
     )
     outgoing = jnp.dot(placing, normed, preferred_element_type=jnp.float32).astype(jnp.bfloat16)
-    outgoing = outgoing.reshape(experts, capacity, D)
-    gate_mat = expert_gate[0]
-    up_mat = expert_up[0]
-    down_mat = expert_down[0]
-    slots = lax.all_to_all(outgoing, ("sp", "tp"), split_axis=0, concat_axis=0, tiled=True)
-    flat_rows = slots.reshape(-1, slots.shape[-1])
-    gate_pre = jnp.dot(flat_rows, gate_mat, preferred_element_type=jnp.float32)
-    up_pre = jnp.dot(flat_rows, up_mat, preferred_element_type=jnp.float32)
-    expert_act = (jax.nn.silu(gate_pre) * up_pre).astype(jnp.bfloat16)
-    done = jnp.dot(expert_act, down_mat, preferred_element_type=jnp.float32).astype(jnp.bfloat16)
-    answered = done.reshape(slots.shape)
-    returned = lax.all_to_all(answered, ("sp", "tp"), split_axis=0, concat_axis=0, tiled=True)
-    picked = jnp.take(returned.reshape(experts * capacity, D), target, axis=0).reshape(
-        row_count, top_count, D
+    places = jnp.arange(experts * capacity, dtype=jnp.int32)
+    pick = target.reshape(row_count, top_count).T[:, :, None] == places
+    return moe(
+        mesh, capacity, outgoing, stream, pick.astype(jnp.bfloat16), route_weight,
+        expert_gate, expert_up, expert_down,
     )
-    combined = jnp.sum(picked.astype(jnp.float32) * route_weight[:, :, None], axis=1)
-    return (stream.astype(jnp.float32) + combined).astype(jnp.bfloat16)
 
 
 def solution(mesh):

time: 170 us -> 152 us (0.89)
  the two profiles are of different devices: /device:TPU:0 before, /device:TPU:16 now
where the time goes in v2:
time: 152 us; the launch traced here: 151 us
  Pallas kernels  135 us (89%)
  local copies, waits for them, and re-layouts  7.62 us (5%)
  matrix products  5.13 us (3%)
  other arithmetic  3.86 us (3%)
    pallas_call x1, Pallas kernels, moe(): pl.pallas_call(functools.partial(moe_kernel, count, ntp, cap), out_shape=...  105 us
    pallas_call x1, Pallas kernels, attend(): pl.pallas_call(functools.partial(attend_kernel, n, nz, nx, ntp, group), o...  29.7 us
    unnamed x17, local copies, waits for them, and re-layouts  6.88 us

profile of v2, /device:TPU:16, one launch (start us, length us, event | category | flops | bytes accessed | tf_op | source)
XLA Modules:
  0.0 151.5 jit_solution(69884216899318785)
XLA Ops:
  0.1 0.1 mul.73
  0.2 0.1 select_convert_fusion.ones_ref
  0.3 0.8 copy.40
  1.1 0.1 eq.101
  1.3 0.1 eq.97
  1.4 0.6 reduce-window.6
  2.0 0.2 slice_reduce_fusion
  2.2 0.1 fusion.12
  2.3 0.1 reduce_sum.30
  2.5 0.1 copy.43
  2.6 0.7 fusion.18
  3.3 0.1 fusion.6
  3.3 1.4 copy.44.share_w
  4.7 0.8 fusion.7.pick
  5.5 1.0 fusion.8
  6.6 0.9 copy-done
  7.5 0.9 copy-done.1
  8.4 0.9 copy-done.2
  9.3 29.7 %attend.1 = bf16[128,1024]{1,0:T(8,128)(2,1)S(1)} custom-call(bf16[512,256]{1,0:T(8,128)(2,1)S(1)} %copy-done, bf16[512,128]{1,0:T(8,128)(2,1)S(1)} %copy-done.1, bf16[512,128]{1,0:T(8,128)(2,1)S(1)} %copy-done.2, f32[512,128]{1,0:T(8,128)S(1)} %get-tuple-element.8.cos_ref, f32[512,128]{1,0:T(8,128)S(1)} %get-tuple-element.7.sin_ref, ...), custom_call_target="tpu_custom_call" | custom-call | tf_op jit(solution)/shard_map/attend/pallas_call | solution.py:225
  39.1 3.0 %multiply_reduce_fusion = (f32[128]{0:T(128)S(1)}, f32[128,2048]{1,0:T(8,128)S(1)}) fusion(bf16[128,1024]{1,0:T(8,128)(2,1)S(1)} %attend.1, bf16[1024,2048]{1,0:T(8,128)(2,1)} %param.16), kind=kOutput, calls=%fused_computation.7 | convolution fusion | flops 537395072 | bytes 5505536 | tf_op jit(solution)/shard_map/dot_general | solution.py:394
  42.1 0.4 fusion
  42.5 2.1 %convolution_convert_fusion.tx = bf16[512,2048]{1,0:T(8,128)(2,1)} fusion(pred[512,128]{1,0:T(8,128)(4,1)S(1)} %fusion.6, bf16[128,2048]{1,0:T(8,128)(2,1)S(1)} %get-tuple-element.6.stream, f32[2048]{0:T(1024)S(1)} %copy-done.6, f32[128]{0:T(128)S(1)} %add_rsqrt_fusion), kind=kOutput, calls=%fused_computation | convolution fusion | flops 270532608 | bytes 2695680 | tf_op jit(solution)/shard_map/dot_general | solution.py:415
  44.6 104.9 %moe.1 = bf16[128,2048]{1,0:T(8,128)(2,1)} custom-call(bf16[512,2048]{1,0:T(8,128)(2,1)} %convolution_convert_fusion.tx, bf16[128,2048]{1,0:T(8,128)(2,1)} %copy-done.3, bf16[2,128,512]{2,1,0:T(8,128)(2,1)} %fusion.7.pick, f32[128,2]{1,0:T(8,128)} %copy.44.share_w, bf16[1,2048,1024]{2,1,0:T(8,128)(2,1)} %gate_hbm.1, bf16[1,2048,1024]{2,1,0:T(8,128)(2,1)} %up_hbm.1, ...), custom_call_target="tpu_custom_call" | custom-call | tf_op jit(solution)/shard_map/moe/pallas_call | solution.py:355
  149.6 1.9 %copy.48 = bf16[128,2048]{1,0:T(8,128)(2,1)} copy(bf16[128,2048]{1,0:T(8,128)(2,1)} %moe.1) | data formatting | bytes 1048576
  (24 shorter events, 0.1 us)
Async XLA Ops:
  0.2 41.9 %copy-start.4 = (bf16[128,2048]{1,0:T(8,128)(2,1)S(1)}, bf16[128,2048]{1,0:T(8,128)(2,1)}, u32[]{:S(2)}) copy-start(bf16[128,2048]{1,0:T(8,128)(2,1)} %param.15) | copy-start | bytes 1572868
  0.2 41.9 %copy-start.5 = (f32[2048]{0:T(1024)S(1)}, f32[2048]{0:T(1024)}, u32[]{:S(2)}) copy-start(f32[2048]{0:T(1024)} %param.17) | copy-start | bytes 24580
  6.6 1.0 copy-start
  7.5 0.9 copy-start.1
  8.4 0.9 copy-start.2
  9.3 33.2 %copy-start.6 = (f32[2048]{0:T(1024)S(1)}, f32[2048]{0:T(1024)}, u32[]{:S(2)}) copy-start(f32[2048]{0:T(1024)} %param.18) | copy-start | bytes 24580
  42.5 2.2 %copy-start.3 = (bf16[128,2048]{1,0:T(8,128)(2,1)}, bf16[128,2048]{1,0:T(8,128)(2,1)S(1)}, u32[]{:S(2)}) copy-start(bf16[128,2048]{1,0:T(8,128)(2,1)S(1)} %get-tuple-element.6.stream) | copy-start | bytes 1572868

commit v3 on v2

--- a/solution.py
+++ b/solution.py
@@ -38,13 +38,20 @@
 
 def attend_kernel(
     n, nz, nx, ntp, group,
-    q_ref, k_ref, v_ref, cos_ref, sin_ref, swap_ref, ones_ref,
+    q_hbm, k_hbm, v_hbm, cos_ref, sin_ref, swap_ref, ones_ref,
     out_ref,
-    qs, acc, fb, bb, att, rx,
-    send_f, recv_f, send_b, recv_b, send_t, recv_t,
+    q_ref, k_ref, v_ref, qs, acc, fb, bb, att, rx,
+    load_sem, send_f, recv_f, send_b, recv_b, send_t, recv_t,
 ):
     sp = lax.axis_index("sp")
     tp = lax.axis_index("tp")
+    loads = [
+        pltpu.make_async_copy(k_hbm, k_ref, load_sem.at[0]),
+        pltpu.make_async_copy(v_hbm, v_ref, load_sem.at[1]),
+        pltpu.make_async_copy(q_hbm, q_ref, load_sem.at[2]),
+    ]
+    for load in loads:
+        load.start()
     toks = q_ref.shape[0]
     heads = q_ref.shape[1] // HEAD_SIZE
     half = toks // 2
@@ -75,6 +82,8 @@
         partner = jnp.dot(block, swap_ref[...], preferred_element_type=jnp.float32)
         return (wide * cos + partner * sin) * lax.rsqrt(mean + epsilon)
 
+    loads[0].wait()
+    loads[1].wait()
     keys = prepare(k_ref[...]).astype(jnp.bfloat16)
     vals = v_ref[...]
     for c in range(2):
@@ -103,6 +112,7 @@
         forward(i).start()
         backward(i).start()
 
+    loads[2].wait()
     scale = HEAD_SIZE ** (-0.5)
     for t in range(heads // 2):
         ready = prepare(q_ref[:, t * LANES : (t + 1) * LANES]) * scale
@@ -225,15 +235,20 @@
     return pl.pallas_call(
         functools.partial(attend_kernel, n, nz, nx, ntp, group),
         out_shape=jax.ShapeDtypeStruct((share, ntp * width), jnp.bfloat16),
-        in_specs=[pl.BlockSpec(memory_space=pltpu.VMEM)] * 7,
+        in_specs=[pl.BlockSpec(memory_space=pltpu.HBM)] * 3
+        + [pl.BlockSpec(memory_space=pltpu.VMEM)] * 4,
         out_specs=pl.BlockSpec(memory_space=pltpu.VMEM),
         scratch_shapes=[
+            pltpu.VMEM(query_proj.shape, jnp.bfloat16),
+            pltpu.VMEM(projected_keys.shape, jnp.bfloat16),
+            pltpu.VMEM(projected_keys.shape, jnp.bfloat16),
             pltpu.VMEM((heads * toks, LANES), jnp.bfloat16),
             pltpu.VMEM((heads * toks, LANES), jnp.float32),
             pltpu.VMEM((n + 1, 2, toks // 2, LANES), jnp.bfloat16),
             pltpu.VMEM((n + 1, 2, toks // 2, LANES), jnp.bfloat16),
             pltpu.VMEM((ntp, share, width), jnp.bfloat16),
             pltpu.VMEM((ntp, share, width), jnp.bfloat16),
+            dma((3,)),
             dma((n - 1,)), dma((n - 1,)), dma((n - 1,)), dma((n - 1,)),
             dma((ntp,)), dma((ntp,)),
         ],

time: 152 us -> 152 us (level)
  no operation moved by 1% of the time
where the time goes in v3:
time: 152 us
  Pallas kernels  135 us (89%)
  local copies, waits for them, and re-layouts  7.62 us (5%)
  matrix products  5.13 us (3%)
  other arithmetic  3.86 us (3%)
    pallas_call x1, Pallas kernels, moe(): pl.pallas_call(functools.partial(moe_kernel, count, ntp, cap), out_shape=...  105 us
    pallas_call x1, Pallas kernels, attend(): pl.pallas_call(functools.partial(attend_kernel, n, nz, nx, ntp, group), o...  30.1 us
    unnamed x17, local copies, waits for them, and re-layouts  6.88 us

profile of v3, /device:TPU:16, one launch (start us, length us, event | category | flops | bytes accessed | tf_op | source)
XLA Modules:
  0.0 151.9 jit_solution(7446359149590124979)
XLA Ops:
  0.1 0.1 mul.73
  0.2 0.1 select_convert_fusion.ones_ref
  0.3 0.8 copy.40
  1.1 0.1 eq.101
  1.3 0.1 eq.97
  1.4 0.6 reduce-window.6
  2.0 0.2 slice_reduce_fusion
  2.2 0.1 fusion.12
  2.3 0.1 reduce_sum.30
  2.5 0.1 copy.43
  2.6 0.7 fusion.18
  3.3 0.1 fusion.6
  3.3 1.4 copy.44.share_w
  4.7 0.8 fusion.7.pick
  5.5 1.0 fusion.8
  6.6 0.9 copy-done
  7.5 0.9 copy-done.1
  8.4 0.9 copy-done.2
  9.3 30.1 %attend.1 = bf16[128,1024]{1,0:T(8,128)(2,1)S(1)} custom-call(bf16[512,256]{1,0:T(8,128)(2,1)S(1)} %copy-done, bf16[512,128]{1,0:T(8,128)(2,1)S(1)} %copy-done.1, bf16[512,128]{1,0:T(8,128)(2,1)S(1)} %copy-done.2, f32[512,128]{1,0:T(8,128)S(1)} %get-tuple-element.8.cos_ref, f32[512,128]{1,0:T(8,128)S(1)} %get-tuple-element.7.sin_ref, ...), custom_call_target="tpu_custom_call" | custom-call | tf_op jit(solution)/shard_map/attend/pallas_call | solution.py:235
  39.5 3.0 %multiply_reduce_fusion = (f32[128]{0:T(128)S(1)}, f32[128,2048]{1,0:T(8,128)S(1)}) fusion(bf16[128,1024]{1,0:T(8,128)(2,1)S(1)} %attend.1, bf16[1024,2048]{1,0:T(8,128)(2,1)} %param.16), kind=kOutput, calls=%fused_computation.7 | convolution fusion | flops 537395072 | bytes 5505536 | tf_op jit(solution)/shard_map/dot_general | solution.py:409
  42.5 0.4 fusion
  42.9 2.1 %convolution_convert_fusion.tx = bf16[512,2048]{1,0:T(8,128)(2,1)} fusion(pred[512,128]{1,0:T(8,128)(4,1)S(1)} %fusion.6, bf16[128,2048]{1,0:T(8,128)(2,1)S(1)} %get-tuple-element.6.stream, f32[2048]{0:T(1024)S(1)} %copy-done.6, f32[128]{0:T(128)S(1)} %add_rsqrt_fusion), kind=kOutput, calls=%fused_computation | convolution fusion | flops 270532608 | bytes 2695680 | tf_op jit(solution)/shard_map/dot_general | solution.py:430
  45.0 105.0 %moe.1 = bf16[128,2048]{1,0:T(8,128)(2,1)} custom-call(bf16[512,2048]{1,0:T(8,128)(2,1)} %convolution_convert_fusion.tx, bf16[128,2048]{1,0:T(8,128)(2,1)} %copy-done.3, bf16[2,128,512]{2,1,0:T(8,128)(2,1)} %fusion.7.pick, f32[128,2]{1,0:T(8,128)} %copy.44.share_w, bf16[1,2048,1024]{2,1,0:T(8,128)(2,1)} %gate_hbm.1, bf16[1,2048,1024]{2,1,0:T(8,128)(2,1)} %up_hbm.1, ...), custom_call_target="tpu_custom_call" | custom-call | tf_op jit(solution)/shard_map/moe/pallas_call | solution.py:370
  150.0 1.9 %copy.48 = bf16[128,2048]{1,0:T(8,128)(2,1)} copy(bf16[128,2048]{1,0:T(8,128)(2,1)} %moe.1) | data formatting | bytes 1048576
  (24 shorter events, 0.1 us)
Async XLA Ops:
  0.2 42.3 %copy-start.4 = (bf16[128,2048]{1,0:T(8,128)(2,1)S(1)}, bf16[128,2048]{1,0:T(8,128)(2,1)}, u32[]{:S(2)}) copy-start(bf16[128,2048]{1,0:T(8,128)(2,1)} %param.15) | copy-start | bytes 1572868
  0.2 42.3 %copy-start.5 = (f32[2048]{0:T(1024)S(1)}, f32[2048]{0:T(1024)}, u32[]{:S(2)}) copy-start(f32[2048]{0:T(1024)} %param.17) | copy-start | bytes 24580
  6.6 1.0 copy-start
  7.5 0.9 copy-start.1
  8.4 0.9 copy-start.2
  9.3 33.6 %copy-start.6 = (f32[2048]{0:T(1024)S(1)}, f32[2048]{0:T(1024)}, u32[]{:S(2)}) copy-start(f32[2048]{0:T(1024)} %param.18) | copy-start | bytes 24580
  42.9 2.2 %copy-start.3 = (bf16[128,2048]{1,0:T(8,128)(2,1)}, bf16[128,2048]{1,0:T(8,128)(2,1)S(1)}, u32[]{:S(2)}) copy-start(bf16[128,2048]{1,0:T(8,128)(2,1)S(1)} %get-tuple-element.6.stream) | copy-start | bytes 1572868
